TPU v7x, 128 devices: a whole 4x4x4 slice. The times are simulated.
128 devices in a mesh: ep: 16 (over z, x), tp: 8 (over y, core).
Axes of the slice: x: 4, y: 4, z: 4, core: 2. Of those that a mesh axis runs over, the one named last changes fastest.
Arguments:
- tokens: bfloat16 [16384, 2048], P(('ep', 'tp')), may hold values from -6 to 6
- expert_ids: int32 [16384, 4], P('ep'), may hold values from 0 to 15, all different within a row; in each aligned block of 128 rows (0 to 127, 128 to 255, ...) at most 64 rows name the same one
- gate_values: float32 [16384, 4], P('ep'), may hold values from 0.1 to 1
- norm_gain: float32 [2048], replicated, may hold values from 0.1 to 1.9
- gate_weight: bfloat16 [16, 2048, 1024], P('ep', None, 'tp'), may hold values from -0.125 to 0.125
- up_weight: bfloat16 [16, 2048, 1024], P('ep', None, 'tp'), may hold values from -0.125 to 0.125
- down_weight: bfloat16 [16, 1024, 2048], P('ep', 'tp'), may hold values from -0.1875 to 0.1875
- out_gain: float32 [2048], P('tp'), may hold values from 0.1 to 1.9
Outputs:
- mixed: bfloat16 [16384, 2048], P('ep', 'tp')
Inputs may be any that keep to these rules, and one draw needn't show every extreme that they name: `expert_ids`: each row names 4 different experts of 0 to 15; within the rows of one device (aligned blocks of 128 rows) no expert is named more than 64 times, and in some blocks one expert is named exactly 64 times.
All inputs are finite; a program needn't handle non-finite values.
Results may differ from a plain program's by a relative error of at most 0.0025.
Values may be sent and summed in bfloat16 or wider, within the bound.
A program may use at most 64 MiB of HBM per device.

v0:
```python
import jax
import jax.numpy as jnp
from jax import lax
from jax.sharding import PartitionSpec as P

epsilon = 1e-05
clamp_limit = 7.0
sigmoid_alpha = 1.702


def taken_in(shard, axis, dim, absorb, state):
    everything = jax.tree.map(lambda a: lax.all_gather(a, axis, axis=dim, tiled=True), shard)
    return absorb(state, everything, jnp.int32(0))


def rms_rows(values, gain):
    mean_sq = jnp.mean(values * values, axis=-1, keepdims=True)
    return values * lax.rsqrt(mean_sq + epsilon) * gain


def clamped_unit(gate_part, up_part):
    glu_part = jnp.minimum(gate_part, clamp_limit)
    lin_part = jnp.clip(up_part, -clamp_limit, clamp_limit)
    return glu_part * jax.nn.sigmoid(sigmoid_alpha * glu_part) * (lin_part + 1.0)


def local(
    tokens, expert_ids, gate_values, norm_gain, gate_weight, up_weight, down_weight, out_gain
):
    expert_groups = lax.axis_size("ep")
    width_groups = lax.axis_size("tp")
    tok_rows = tokens.shape[0]
    model_width = tokens.shape[1]
    top_count = expert_ids.shape[1]
    capacity = tok_rows // 2
    per_rank = capacity // width_groups
    slice_w = model_width // width_groups
    normed = rms_rows(tokens.astype(jnp.float32), norm_gain).astype(jnp.bfloat16)
    blocks = expert_ids.reshape(width_groups, tok_rows * top_count)
    onehot = (
        blocks[:, :, None] == jnp.arange(expert_groups, dtype=jnp.int32)[None, None, :]
    ).astype(jnp.int32)
    slot_num = jnp.sum((jnp.cumsum(onehot, axis=1) - onehot) * onehot, axis=2)
    own_rank = lax.axis_index("tp")
    own_ids = lax.dynamic_index_in_dim(blocks, own_rank, 0, keepdims=False)
    own_slots = lax.dynamic_index_in_dim(slot_num, own_rank, 0, keepdims=False)
    target = own_ids * capacity + own_slots
    entry_token = jnp.arange(tok_rows * top_count, dtype=jnp.int32) // top_count
    owner_row = (
        jnp.full((expert_groups * capacity,), tok_rows, jnp.int32).at[target].set(entry_token)
    )
    padded = jnp.concatenate([normed, jnp.zeros((1, model_width), jnp.bfloat16)], axis=0)
    outgoing = padded[owner_row].reshape(expert_groups * width_groups, per_rank, model_width)
    arrived = lax.all_to_all(outgoing, ("ep", "tp"), split_axis=0, concat_axis=0, tiled=True)
    arrived_rows = arrived.reshape(-1, model_width)
    row_total = arrived_rows.shape[0]
    hidden_width = gate_weight.shape[2] * width_groups
    blank_acts = jnp.zeros((row_total, hidden_width), jnp.bfloat16)

    def add_hidden(activated, pieces, offset):
        gate_part = jnp.dot(arrived_rows, pieces[0][0], preferred_element_type=jnp.float32)
        up_part = jnp.dot(arrived_rows, pieces[1][0], preferred_element_type=jnp.float32)
        fresh = clamped_unit(gate_part, up_part).astype(jnp.bfloat16)
        return lax.dynamic_update_slice_in_dim(activated, fresh, offset, 1)

    activated = taken_in((gate_weight, up_weight), "tp", 2, add_hidden, blank_acts)

    def add_output(running, w_piece, offset):
        act_part = lax.dynamic_slice_in_dim(activated, offset, w_piece.shape[1], 1)
        return running + jnp.dot(act_part, w_piece[0], preferred_element_type=jnp.float32)

    blank_out = jnp.zeros((row_total, model_width), jnp.float32)
    result = taken_in(down_weight, "tp", 1, add_output, blank_out).astype(jnp.bfloat16)
    outbound = result.reshape(expert_groups, width_groups, per_rank, width_groups, slice_w)
    outbound = outbound.transpose(0, 3, 1, 2, 4)
    landed = lax.all_to_all(
        outbound.reshape(expert_groups * width_groups, width_groups, per_rank, slice_w),
        ("ep", "tp"),
        split_axis=0,
        concat_axis=0,
        tiled=True,
    )
    returned = landed.reshape(-1, slice_w)
    rank_part = slot_num // per_rank
    within = slot_num % per_rank
    source_col = jnp.arange(width_groups, dtype=jnp.int32)[:, None]
    row_index = (
        (blocks * width_groups + rank_part) * width_groups + source_col
    ) * per_rank + within
    picked = returned[row_index.reshape(-1)].astype(jnp.float32)
    picked = picked.reshape(width_groups * tok_rows, top_count, slice_w)
    combined = jnp.sum(gate_values[:, :, None] * picked, axis=1)
    local_sq = jnp.sum(combined * combined, axis=1)
    total_sq = lax.psum(local_sq, "tp")
    row_scale = lax.rsqrt(total_sq / model_width + epsilon)
    return (combined * row_scale[:, None] * out_gain).astype(jnp.bfloat16)


def solution(mesh):
    in_specs = (
        P(("ep", "tp"), None),
        P("ep", None),
        P("ep", None),
        P(),
        P("ep", None, "tp"),
        P("ep", None, "tp"),
        P("ep", "tp", None),
        P("tp"),
    )
    out_specs = P("ep", "tp")
    return jax.shard_map(local, mesh=mesh, in_specs=in_specs, out_specs=out_specs, check_vma=False)
```

profile of v0, /device:TPU:2, one launch (start us, length us, event | category | flops | bytes accessed | tf_op | source)
XLA Modules:
  0.0 275.4 jit_solution(7951599097116689879)
XLA Ops:
  6.5 0.0 copy-start
  6.5 0.0 copy-start.3
  6.5 0.0 all-gather.6.cloned.1.call-start
  6.5 0.7 all-gather.6.cloned.1.call-update
  7.3 0.0 all-gather.4.cloned.1.call-start
  7.3 0.7 all-gather.4.cloned.1.call-update
  8.0 0.0 all-gather.8.cloned.1.call-start
  8.1 0.7 all-gather.8.cloned.1.call-update
  8.7 0.9 copy.11
  9.7 0.3 eq.28
  10.0 0.3 reshape.220
  10.3 9.1 %reduce-window.6 = s32[8,16,4,128]{3,1,2,0:T(8,128)S(1)} reduce-window(s32[8,16,4,128]{3,1,2,0:T(8,128)S(1)} %fusion.21, s32[]{:T(128)} %constant.77.clone.1), window={size=1x1x1x128 pad=0_0x0_0x0_0x127_0}, to_apply=%region_1.0 | reduce-window | flops 8323072 | bytes 524292 | tf_op jit(solution)/shard_map/reduce-window
  19.4 0.1 slice.12
  19.5 0.3 copy.13
  19.8 0.1 fusion.23
  19.9 0.0 copy-done
  19.9 0.2 fusion.15
  20.1 0.0 copy-done.3
  20.1 0.2 fusion.17
  20.4 0.1 fusion.20
  20.6 2.4 scatter_custom_fusion
  23.0 6.0 %gather_fusion = bf16[1024,2048]{1,0:T(8,128)(2,1)} fusion(bf16[129,2048]{1,0:T(8,128)(2,1)S(1)} %concatenate.3, s32[1024]{0:T(1024)S(1)} %fusion.25), kind=kCustom, calls=%fused_computation | custom fusion | bytes 8392704 | tf_op jit(solution)/shard_map/gather | solution.py:53
  29.1 65.6 %all_to_all.10 = bf16[128,8,2048]{2,1,0:T(8,128)(2,1)} all-to-all(bf16[128,8,2048]{2,1,0:T(8,128)(2,1)} %bitcast.62), channel_id=1, replica_groups=mesh['ep'=16,'tp'=8] {'ep','tp'}, dimensions={0} | all-to-all | bytes 8388608 | tf_op jit(solution)/shard_map/all_to_all | solution.py:54
  94.7 0.0 all-gather.6.cloned.1.call-done
  94.7 9.9 %fusion.2 = f32[1024,1024]{1,0:T(8,128)} fusion(bf16[1,2048,1024]{2,1,0:T(8,128)(2,1)} %all-gather.6.cloned.1.call-done, bf16[128,8,2048]{2,1,0:T(8,128)(2,1)} %all_to_all.10), kind=kOutput, calls=%fused_computation.5 | convolution fusion | flops 4294967296 | bytes 12582912 | tf_op jit(solution)/shard_map/dot_general | solution.py:62
  104.5 10.1 %all-gather.4.cloned.1.call-done = bf16[1,2048,1024]{2,1,0:T(8,128)(2,1)} async-done(((bf16[1,2048,128]{2,1,0:T(8,128)(2,1)}), bf16[1,2048,1024]{2,1,0:T(8,128)(2,1)}) %all-gather.4.cloned.1.call-update) | async-done | bytes 4194320 | tf_op jit(solution)/shard_map/all_gather | solution.py:12
  114.7 10.1 %multiply_convert_fusion = bf16[1024,1024]{1,0:T(8,128)(2,1)S(1)} fusion(f32[1024,1024]{1,0:T(8,128)} %fusion.2, bf16[1,2048,1024]{2,1,0:T(8,128)(2,1)} %all-gather.4.cloned.1.call-done, bf16[128,8,2048]{2,1,0:T(8,128)(2,1)} %all_to_all.10), kind=kOutput, calls=%fused_computation.12 | convolution fusion | flops 4305453056 | bytes 14680064 | tf_op jit(solution)/shard_map/dot_general | solution.py:61
  124.7 24.0 %all-gather.8.cloned.1.call-done = bf16[1,1024,2048]{2,1,0:T(8,128)(2,1)} async-done(((bf16[1,128,2048]{2,1,0:T(8,128)(2,1)}), bf16[1,1024,2048]{2,1,0:T(8,128)(2,1)}) %all-gather.8.cloned.1.call-update) | async-done | bytes 4194320 | tf_op jit(solution)/shard_map/all_gather | solution.py:12
  148.7 6.9 %fusion.8 = bf16[1024,2048]{1,0:T(8,128)(2,1)S(1)} fusion(bf16[1024,1024]{1,0:T(8,128)(2,1)S(1)} %multiply_convert_fusion, bf16[1,1024,2048]{2,1,0:T(8,128)(2,1)} %all-gather.8.cloned.1.call-done), kind=kOutput, calls=%fused_computation.13 | convolution fusion | flops 4297064448 | bytes 10485760 | tf_op jit(solution)/shard_map/dot_general | solution.py:70
  155.6 2.6 copy.16
  158.1 0.0 copy-start.1
  158.1 0.0 copy-start.2
  158.1 8.6 %all-to-all-start.1 = ((bf16[128,8,8,256]{3,2,1,0:T(8,128)(2,1)}), bf16[128,8,8,256]{3,2,1,0:T(8,128)(2,1)}, u32[]{:S(2)}, u32[]{:S(2)}) async-start(bf16[128,8,8,256]{3,2,1,0:T(8,128)(2,1)} %bitcast.63), calls=%async_computation.1 | async-start | bytes 8388608 | tf_op jit(solution)/shard_map/all_to_all | solution.py:76
  166.8 0.0 copy-done.1
  166.8 0.2 copy.17
  167.0 0.3 mul.125
  167.4 0.0 copy-done.2
  167.4 0.2 copy.10
  167.6 0.2 compare_select_fusion
  167.8 59.0 %all-to-all-done.1 = bf16[128,8,8,256]{3,2,1,0:T(8,128)(2,1)} async-done(((bf16[128,8,8,256]{3,2,1,0:T(8,128)(2,1)}), bf16[128,8,8,256]{3,2,1,0:T(8,128)(2,1)}, u32[]{:S(2)}, u32[]{:S(2)}) %all-to-all-start.1) | async-done | bytes 4194336 | tf_op jit(solution)/shard_map/all_to_all | solution.py:76
  226.8 15.7 %gather_fusion.1 = bf16[4096,256]{1,0:T(8,128)(2,1)S(1)} fusion(bf16[8192,256]{1,0:T(8,128)(2,1)} %bitcast.12, s32[4096]{0:T(1024)S(1)} %broadcast_clamp_fusion), kind=kCustom, calls=%fused_computation.1 | custom fusion | bytes 4210688 | tf_op jit(solution)/shard_map/gather | solution.py:90
  242.6 2.9 %reshape.227 = f32[1024,4,256]{2,1,0:T(4,128)} reshape(bf16[4096,256]{1,0:T(8,128)(2,1)S(1)} %gather_fusion.1) | data formatting | bytes 6291456 | tf_op jit(solution)/shard_map/convert_element_type | solution.py:90
  245.4 0.0 copy-start.4
  245.4 7.2 %multiply_reduce_fusion = f32[1024,256]{1,0:T(8,128)S(1)} fusion(f32[1024,4,256]{2,1,0:T(4,128)} %reshape.227, f32[1024,4]{1,0:T(8,128)S(1)} %copy.10), kind=kLoop, calls=%fused_computation.11 | loop fusion | flops 1835008 | bytes 5259264 | tf_op jit(solution)/shard_map/reduce_sum | solution.py:92
  252.6 0.2 multiply_reduce_fusion.1
  252.8 15.0 %psum.7 = f32[1024]{0:T(1024)S(1)} all-reduce(f32[1024]{0:T(1024)S(1)} %multiply_reduce_fusion.1), channel_id=1, replica_groups=mesh['ep'=16,'tp'=8] {'tp'}, use_global_device_ids=true, to_apply=%region_7.8 | all-reduce | flops 1024 | bytes 8192 | tf_op jit(solution)/shard_map/psum | solution.py:94
  267.9 0.0 copy-done.4
  267.9 1.0 multiply_convert_fusion.1
  (14 shorter events, 0.2 us)
Async XLA Ops:
  6.5 13.4 %copy-start = (bf16[128,2048]{1,0:T(8,128)(2,1)S(1)}, bf16[128,2048]{1,0:T(8,128)(2,1)}, u32[]{:S(2)}) copy-start(bf16[128,2048]{1,0:T(8,128)(2,1)} %param.8) | copy-start | bytes 1572868
  6.5 13.6 %copy-start.3 = (f32[2048]{0:T(1024)S(1)}, f32[2048]{0:T(1024)}, u32[]{:S(2)}) copy-start(f32[2048]{0:T(1024)} %param.11) | copy-start | bytes 24580
  6.5 88.1 %all-gather.6.cloned.1.call-start = ((), (), s32[]{:S(2)}) async-start(), calls=%async_computation.3 | async-start | bytes 4718592 | tf_op jit(solution)/shard_map/all_gather | solution.py:12
  7.3 107.4 %all-gather.4.cloned.1.call-start = ((), (), s32[]{:S(2)}) async-start(), calls=%async_computation.2 | async-start | bytes 4718592 | tf_op jit(solution)/shard_map/all_gather | solution.py:12
  8.0 140.7 %all-gather.8.cloned.1.call-start = ((), (), s32[]{:S(2)}) async-start(), calls=%async_computation.4 | async-start | bytes 4718592 | tf_op jit(solution)/shard_map/all_gather | solution.py:12
  158.1 8.6 %copy-start.1 = (s32[1024,4]{0,1:T(4,128)S(1)}, s32[1024,4]{0,1:T(4,128)}, u32[]{:S(2)}) copy-start(s32[1024,4]{0,1:T(4,128)} %param.9) | copy-start | bytes 49156
  158.1 9.2 %copy-start.2 = (f32[1024,4]{0,1:T(4,128)S(1)}, f32[1024,4]{0,1:T(4,128)}, u32[]{:S(2)}) copy-start(f32[1024,4]{0,1:T(4,128)} %param.10) | copy-start | bytes 49156
  158.1 68.7 %all-to-all-start.1 = ((bf16[128,8,8,256]{3,2,1,0:T(8,128)(2,1)}), bf16[128,8,8,256]{3,2,1,0:T(8,128)(2,1)}, u32[]{:S(2)}, u32[]{:S(2)}) async-start(bf16[128,8,8,256]{3,2,1,0:T(8,128)(2,1)} %bitcast.63), calls=%async_computation.1 | async-start | bytes 8388608 | tf_op jit(solution)/shard_map/all_to_all | solution.py:76
  245.4 22.5 %copy-start.4 = (f32[256]{0:T(256)S(1)}, f32[256]{0:T(256)}, u32[]{:S(2)}) copy-start(f32[256]{0:T(256)} %param.15) | copy-start | bytes 3076
Sparse Core Ops, SparseCore 0:
  9.0 47.9 all-gather.5
  58.7 55.9 all-gather.3
  116.4 32.2 all-gather.7
where the time goes:
time: 276 us; the launch traced here: 275 us
  waiting for transfers between devices  95.2 us (34%)
  blocking collectives  80.6 us (29%)
  local copies, waits for them, and re-layouts  32.4 us (12%)
  matrix products  26.8 us (10%)
  other arithmetic  18.3 us (7%)
  between operations  13.4 us (5%)
  starting transfers between devices  8.66 us (3%)
    all_to_all x1, blocking collectives, local(): lax.all_to_all(outgoing, ('ep', 'tp'), split_axis=0, concat_axis=0, tiled...  65.6 us
    all_to_all x1, waiting for transfers between devices, local(): lax.all_to_all(outbound.reshape(expert_groups * width_groups, width_group...  59 us
    all_gather x3, waiting for transfers between devices, taken_in(): lax.all_gather(a, axis, axis=dim, tiled=True)  34.1 us
    gather x1, local copies, waits for them, and re-layouts, local(): picked = returned[row_index.reshape(-1)].astype(jnp.float32)  15.7 us
    psum x1, blocking collectives, local(): total_sq = lax.psum(local_sq, 'tp')  15 us
    dot_general x1, matrix products, add_hidden(): jnp.dot(arrived_rows, pieces[0][0], preferred_element_type=jnp.float32)  10.1 us
    dot_general x1, matrix products, add_hidden(): jnp.dot(arrived_rows, pieces[1][0], preferred_element_type=jnp.float32)  9.87 us
    another operation x2, other arithmetic  9.2 us
  transfers between devices with their start and end apart: 4, of which 3 were waited for; matrix products, arithmetic and copies ran while one was open for 15% of the time, Pallas kernels for 0%

commit v1 on v0

v1 whole, which is shorter than its diff:
```python
import jax
import jax.numpy as jnp
from jax import lax
from jax.experimental import pallas as pl
from jax.experimental.pallas import tpu as pltpu
from jax.sharding import PartitionSpec as P

epsilon = 1e-05
clamp_limit = 7.0
sigmoid_alpha = 1.702

MESH = pl.DeviceIdType.MESH
F32, BF16 = jnp.float32, jnp.bfloat16
D, FF, TOP, TOK, CAP = 2048, 1024, 4, 128, 64
NE, NT = 16, 8
HID = FF // NT
NCH = 4
CW = D // NCH
SL = D // NT
DA = (0, 1, 3, 2)


def clamped_unit(gate_part, up_part):
    glu_part = jnp.minimum(gate_part, clamp_limit)
    lin_part = jnp.clip(up_part, -clamp_limit, clamp_limit)
    return glu_part * jax.nn.sigmoid(sigmoid_alpha * glu_part) * (lin_part + 1.0)


def kernel(
    tok_ref, ids_ref, gv_ref, gain_ref, g_ref, u_ref, d_ref, og_ref,
    out_ref,
    wgu, wd, tb, rt, sel, xr, act, ob, rb, ret, comb, cm, mixed, og,
    w_own, w_s, w_r, d_s, d_r, s1_s, s1_r, s2_s, s2_r, r1_s, r1_r, r2_s, r2_r, g_s, g_r, o_s, o_r, o_l,
):
    ep, tp = lax.axis_index("ep"), lax.axis_index("tp")
    z, x = ep // 4, ep % 4
    y, c = tp // 2, tp % 2
    a = z * (1 - c) + x * c
    b = x * (1 - c) + z * c
    wa, wb = 4 - 3 * c, 1 + 3 * c

    def ab(da, db):
        return (((a + da) % 4) * wa + ((b + db) % 4) * wb, tp)

    def yc(dy, dc):
        return (ep, ((y + dy) % 4) * 2 + (c + dc) % 2)

    def send(src, dst, ss, rs, dev):
        cp = pltpu.make_async_remote_copy(
            src_ref=src, dst_ref=dst, send_sem=ss, recv_sem=rs, device_id=dev, device_id_type=MESH
        )
        return cp

    sent = []

    def go(cp):
        cp.start()
        sent.append(cp)
        return cp

    barrier = pltpu.get_barrier_semaphore()
    peers = [ab(i, 0) for i in (1, 2, 3)] + [ab(0, i) for i in (1, 2, 3)]
    peers += [(ep, (tp + i) % NT) for i in range(1, NT)]
    for peer in peers:
        pl.semaphore_signal(barrier, inc=1, device_id=peer, device_id_type=MESH)
    pl.semaphore_wait(barrier, len(peers))

    def gview(p, i):
        return wgu.at[p, :, pl.ds(i * 256, 128)]

    def uview(p, i):
        return wgu.at[p, :, pl.ds(i * 256 + 128, 128)]

    def dview(j, p, i, lo=0, n=HID):
        return wd.at[j, pl.ds((2 * p + i) * HID + lo, n), :]

    gin, uin = g_ref.at[0], u_ref.at[0]

    def din(j):
        return d_ref.at[0, :, pl.ds(j * CW, CW)]

    def wsem(kind, p, i):
        return kind * 8 + i * 4 + p

    def wcopy(kind, src, p, i, dev, extra=0):
        view = gview if kind == 0 else uview
        k = wsem(kind, p, i)
        return send(src, view(p, i), w_s.at[k], w_r.at[k], dev)

    up1, up2 = yc(1, 0), yc(3, 0)
    sib = yc(0, 1)
    g_up = go(wcopy(0, gin, 2, 0, up1))
    g_dn = go(wcopy(0, gin, 1, 0, up2))
    u_up = go(wcopy(1, uin, 2, 0, up1))
    u_dn = go(wcopy(1, uin, 1, 0, up2))
    g_sib = go(wcopy(0, gin, 0, 1, sib))
    u_sib = go(wcopy(1, uin, 0, 1, sib))
    locs = [
        pltpu.make_async_copy(gin, gview(0, 0), w_own.at[0]),
        pltpu.make_async_copy(uin, uview(0, 0), w_own.at[1]),
    ]
    for j in range(NCH):
        locs.append(pltpu.make_async_copy(din(j), dview(j, 0, 0), w_own.at[2 + j]))
    for cp in locs:
        cp.start()
    ogc = []
    for i in range(1, NT):
        ogc.append(go(send(og_ref, og.at[tp], g_s.at[i - 1], g_r.at[i - 1], (ep, (tp + i) % NT))))
    og[tp] = og_ref[...]

    tf = tok_ref[...].astype(F32)
    ms = jnp.mean(tf * tf, axis=-1, keepdims=True)
    tb[0] = (tf * lax.rsqrt(ms + epsilon) * gain_ref[...]).astype(BF16)

    q = lax.broadcasted_iota(jnp.int32, (NE, TOK), 0)
    eid = ((a + q // 4) % 4) * wa + ((b + q % 4) % 4) * wb
    off = pl.multiple_of(tp * TOK, TOK)
    named = jnp.zeros((NE, TOK), F32)
    weight = jnp.zeros((NE, TOK), F32)
    for k in range(TOP):
        hit = ids_ref[k : k + 1, pl.ds(off, TOK)] == eid
        named = named + jnp.where(hit, 1.0, 0.0)
        weight = weight + jnp.where(hit, gv_ref[k : k + 1, pl.ds(off, TOK)], 0.0)
    tri = lax.broadcasted_iota(jnp.int32, (TOK, TOK), 0) < lax.broadcasted_iota(jnp.int32, (TOK, TOK), 1)
    earlier = jnp.dot(named.astype(BF16), jnp.where(tri, 1.0, 0.0).astype(BF16), preferred_element_type=F32)
    table = jnp.where(named > 0.5, earlier, -1.0)
    rt[0] = table

    s1 = {}
    for n, da in enumerate((1, 3, 2)):
        s1[da] = (
            send(tb.at[0], tb.at[(4 - da) % 4], s1_s.at[2 * n], s1_r.at[2 * ((4 - da) % 4)], ab(da, 0)),
            send(rt.at[0], rt.at[(4 - da) % 4], s1_s.at[2 * n + 1], s1_r.at[2 * ((4 - da) % 4) + 1], ab(da, 0)),
        )
        go(s1[da][1])
        go(s1[da][0])

    slot_iota = lax.broadcasted_iota(jnp.int32, (CAP, TOK), 0).astype(F32)

    s2 = {}

    def select(g):
        da = DA[g]
        rows = tb[da]
        for db in range(4):
            line = rt[da, ((4 - da) % 4) * 4 + db : ((4 - da) % 4) * 4 + db + 1, :]
            pick = jnp.where(line == slot_iota, 1.0, 0.0).astype(BF16)
            got = jnp.dot(pick, rows, preferred_element_type=F32).astype(BF16)
            if db == 0:
                xr[g, 0] = got
            else:
                sel[g, db - 1] = got
        for db in (1, 3, 2):
            k, kr = g * 3 + db - 1, g * 3 + (4 - db) % 4 - 1
            s2[g, db] = go(
                send(sel.at[g, db - 1], xr.at[g, (4 - db) % 4], s2_s.at[k], s2_r.at[kr], ab(0, db))
            )

    select(0)

    pad = jnp.zeros((TOK - NE, TOK), F32)
    table_t = jnp.concatenate([table, pad], axis=0).T[:, :NE]
    weight_t = jnp.concatenate([weight, pad], axis=0).T[:, :NE]
    spread = (
        lax.broadcasted_iota(jnp.int32, (NE, NE * CAP), 1) // CAP
        == lax.broadcasted_iota(jnp.int32, (NE, NE * CAP), 0)
    )
    spread = jnp.where(spread, 1.0, 0.0).astype(BF16)
    slot_of = jnp.dot(table_t.astype(BF16), spread, preferred_element_type=F32)
    lane_slot = (lax.broadcasted_iota(jnp.int32, (TOK, NE * CAP), 1) % CAP).astype(F32)
    here = slot_of == lane_slot
    rest = weight_t
    for i in range(3):
        part = rest.astype(BF16)
        rest = rest - part.astype(F32)
        wide = jnp.dot(part, spread, preferred_element_type=F32)
        cm[i * TOK : (i + 1) * TOK, :] = jnp.where(here, wide, 0.0).astype(BF16)

    def s1_wait(da):
        n = {1: 0, 3: 1, 2: 2}[da]
        for t, buf in ((1, rt), (0, tb)):
            send(buf.at[0], buf.at[da], s1_s.at[2 * n + t], s1_r.at[2 * da + t], ab(da, 0)).wait_recv()

    s1_wait(1)
    select(1)
    s1_wait(3)
    select(2)

    def w_wait(kind, p, i):
        wcopy(kind, gin if kind == 0 else uin, p, i, sib).wait_recv()

    def to_sib(kind, p):
        view = gview if kind == 0 else uview
        go(wcopy(kind, view(p, 0), p, 1, sib))

    def gu(g, p):
        rows = xr[g].reshape(4 * CAP, D)
        h = jnp.dot(rows, wgu[p], preferred_element_type=F32)
        for i in range(2):
            part = clamped_unit(h[:, i * 256 : i * 256 + 128], h[:, i * 256 + 128 : i * 256 + 256])
            act[g, :, pl.ds(pl.multiple_of((2 * p + i) * HID, HID), HID)] = part.astype(BF16)

    def x_wait(g):
        for db in (1, 3, 2):
            s2w = send(sel.at[g, db - 1], xr.at[g, db], s2_s.at[g * 3 + db - 1], s2_r.at[g * 3 + db - 1], ab(0, db))
            s2w.wait_recv()

    w_wait(0, 2, 0)
    go(wcopy(0, gview(2, 0), 3, 0, up1))
    to_sib(0, 2)
    w_wait(0, 1, 0)
    to_sib(0, 1)
    s1_wait(2)
    select(3)

    locs[0].wait()
    locs[1].wait()
    w_wait(0, 0, 1)
    w_wait(1, 0, 1)
    x_wait(0)
    gu(0, 0)

    def dsem(j, p, i):
        return j * 9 + p * 2 + i

    def dcopy(j, src, p, i, dev, lo=0, n=HID):
        k = dsem(j, p, i) if lo == 0 else j * 9 + 8
        return send(src, dview(j, p, i, lo, n), d_s.at[k], d_r.at[k], dev)

    def d_start(j):
        go(dcopy(j, din(j), 2, 0, up1))
        go(dcopy(j, din(j), 1, 0, up2))
        go(dcopy(j, din(j), 0, 1, sib))

    def d_fwd(j):
        dcopy(j, din(j), 2, 0, sib).wait_recv()
        go(dcopy(j, dview(j, 2, 0, 0, 64), 3, 0, up1, 0, 64))
        dcopy(j, din(j), 1, 0, sib).wait_recv()
        go(dcopy(j, dview(j, 1, 0, 64, 64), 3, 0, up2, 64, 64))
        go(dcopy(j, dview(j, 2, 0), 2, 1, sib))
        go(dcopy(j, dview(j, 1, 0), 1, 1, sib))

    def d_last(j):
        dcopy(j, dview(j, 2, 0, 0, 64), 3, 0, sib, 0, 64).wait_recv()
        dcopy(j, dview(j, 1, 0, 64, 64), 3, 0, sib, 64, 64).wait_recv()
        go(dcopy(j, dview(j, 3, 0), 3, 1, sib))

    def d_all(j):
        locs[2 + j].wait()
        for p in range(4):
            dcopy(j, din(j), p, 1, sib).wait_recv()

    w_wait(1, 1, 0)
    go(wcopy(1, uview(1, 0), 3, 0, up2))
    to_sib(1, 1)
    w_wait(1, 2, 0)
    to_sib(1, 2)
    d_start(0)
    d_start(1)
    x_wait(1)
    for p in (1, 2):
        w_wait(0, p, 1)
        w_wait(1, p, 1)

    @pl.loop(1, 3)
    def _(p):
        gu(0, p)

    @pl.loop(0, 3)
    def _(p):
        gu(1, p)

    x_wait(2)

    @pl.loop(0, 3)
    def _(p):
        gu(2, p)

    w_wait(0, 3, 0)
    to_sib(0, 3)
    w_wait(1, 3, 0)
    to_sib(1, 3)
    d_fwd(0)
    d_start(2)
    w_wait(0, 3, 1)
    w_wait(1, 3, 1)

    @pl.loop(0, 3)
    def _(g):
        gu(g, 3)

    x_wait(3)

    @pl.loop(0, 4)
    def _(p):
        gu(3, p)

    def down(j):
        @pl.loop(0, 4)
        def _(g):
            r = jnp.dot(act[g], wd[j], preferred_element_type=F32).astype(BF16).reshape(4, CAP, CW)
            ob[j, g] = r
            rb[j, 0, g] = r[0]

        for db in (1, 3, 2):
            k, kr = j * 3 + db - 1, j * 3 + (4 - db) % 4 - 1
            go(send(ob.at[j, :, db], rb.at[j, (4 - db) % 4], r1_s.at[k], r1_r.at[kr], ab(0, db)))

    def relay(j):
        for db in (1, 3, 2):
            k = j * 3 + db - 1
            send(ob.at[j, :, db], rb.at[j, db], r1_s.at[k], r1_r.at[k], ab(0, db)).wait_recv()
        for g in (1, 2, 3):
            da = DA[g]
            k, kr = j * 3 + da - 1, j * 3 + (4 - da) % 4 - 1
            go(send(rb.at[j, :, g], ret.at[j, (4 - da) % 4], r2_s.at[k], r2_r.at[kr], ab(da, 0)))
        ret[j, 0] = rb[j, :, 0]

    def combine(j):
        for g in (1, 2, 3):
            da = DA[g]
            k = j * 3 + da - 1
            send(rb.at[j, :, g], ret.at[j, da], r2_s.at[k], r2_r.at[k], ab(da, 0)).wait_recv()
        full = jnp.dot(cm[...], ret[j].reshape(NE * CAP, CW), preferred_element_type=F32)
        total = full[0:TOK] + full[TOK : 2 * TOK] + full[2 * TOK : 3 * TOK]
        comb[:, j * CW : (j + 1) * CW] = total
        return jnp.sum(total * total, axis=-1, keepdims=True)

    d_fwd(1)
    d_start(3)
    d_last(0)
    d_all(0)
    down(0)
    d_last(1)
    d_fwd(2)
    d_all(1)
    down(1)
    d_fwd(3)
    d_last(2)
    d_all(2)
    down(2)
    d_last(3)
    d_all(3)
    down(3)
    sq = jnp.zeros((TOK, 1), F32)
    relay(0)
    relay(1)
    for cp in ogc:
        cp.wait_recv()
    relay(2)
    relay(3)
    for j in range(NCH):
        sq = sq + combine(j)
    scale = lax.rsqrt(sq / D + epsilon)
    for t in range(NT):
        mixed[t] = (comb[:, t * SL : (t + 1) * SL] * scale * og[t]).astype(BF16)
    mine = pl.ds(pl.multiple_of(tp * TOK, TOK), TOK)
    outs = []
    for i in range(1, NT):
        to = (tp + i) % NT
        outs.append(go(send(mixed.at[to], out_ref.at[mine, :], o_s.at[i - 1], o_r.at[i - 1], (ep, to))))
    own = pltpu.make_async_copy(mixed.at[tp], out_ref.at[mine, :], o_l)
    own.start()
    for i in range(1, NT):
        frm = (tp + NT - i) % NT
        theirs = pl.ds(pl.multiple_of(frm * TOK, TOK), TOK)
        send(mixed.at[frm], out_ref.at[theirs, :], o_s.at[i - 1], o_r.at[i - 1], (ep, frm)).wait_recv()
    own.wait()
    for cp in sent:
        cp.wait_send()


def local(tokens, expert_ids, gate_values, norm_gain, gate_weight, up_weight, down_weight, out_gain):
    vm = pl.BlockSpec(memory_space=pltpu.VMEM)
    anym = pl.BlockSpec(memory_space=pltpu.HBM)
    dma = pltpu.SemaphoreType.DMA
    return pl.pallas_call(
        kernel,
        out_shape=jax.ShapeDtypeStruct((NT * TOK, SL), BF16),
        in_specs=[vm, vm, vm, vm, anym, anym, anym, vm],
        out_specs=anym,
        scratch_shapes=[
            pltpu.VMEM((4, D, 512), BF16),
            pltpu.VMEM((NCH, FF, CW), BF16),
            pltpu.VMEM((4, TOK, D), BF16),
            pltpu.VMEM((4, NE, TOK), F32),
            pltpu.VMEM((4, 3, CAP, D), BF16),
            pltpu.VMEM((4, 4, CAP, D), BF16),
            pltpu.VMEM((4, 4 * CAP, FF), BF16),
            pltpu.VMEM((NCH, 4, 4, CAP, CW), BF16),
            pltpu.VMEM((NCH, 4, 4, CAP, CW), BF16),
            pltpu.VMEM((NCH, 4, 4, CAP, CW), BF16),
            pltpu.VMEM((TOK, D), F32),
            pltpu.VMEM((3 * TOK, NE * CAP), BF16),
            pltpu.VMEM((NT, TOK, SL), BF16),
            pltpu.VMEM((NT, 1, SL), F32),
            dma((2 + NCH,)), dma((16,)), dma((16,)), dma((NCH * 9,)), dma((NCH * 9,)),
            dma((8,)), dma((8,)), dma((12,)), dma((12,)),
            dma((NCH * 3,)), dma((NCH * 3,)), dma((NCH * 3,)), dma((NCH * 3,)),
            dma((NT - 1,)), dma((NT - 1,)), dma((NT - 1,)), dma((NT - 1,)), dma(()),
        ],
        compiler_params=pltpu.CompilerParams(
            collective_id=0, has_side_effects=True, vmem_limit_bytes=63000000
        ),
    )(
        tokens, expert_ids.T, gate_values.T, norm_gain.reshape(1, D),
        gate_weight, up_weight, down_weight, out_gain.reshape(1, SL),
    )


def solution(mesh):
    in_specs = (
        P(("ep", "tp"), None), P("ep", None), P("ep", None), P(),
        P("ep", None, "tp"), P("ep", None, "tp"), P("ep", "tp", None), P("tp"),
    )
    return jax.shard_map(
        local, mesh=mesh, in_specs=in_specs, out_specs=P("ep", "tp"), check_vma=False
    )
```

time: 276 us -> 121 us (0.44)
  Pallas kernels: 0 us -> 117 us
  waiting for transfers between devices: 95.2 us -> 0 us
  blocking collectives: 80.6 us -> 0 us
  local copies, waits for them, and re-layouts: 32.4 us -> 1.87 us
  matrix products: 26.8 us -> 0 us
  other arithmetic: 18.3 us -> 0 us
  between operations: 13.4 us -> 0.01 us
  starting transfers between devices: 8.66 us -> 0 us
    pallas_call x0 -> x1, Pallas kernels: none -> 117 us  [local(): pl.pallas_call(kernel, out_shape=jax.ShapeDtypeStruct((NT * TOK, SL), BF1...]
    all_to_all x1 -> x0, blocking collectives: 65.6 us -> none  [local(): lax.all_to_all(outgoing, ('ep', 'tp'), split_axis=0, concat_axis=0, tiled...]
    all_to_all x1 -> x0, waiting for transfers between devices: 59 us -> none  [local(): lax.all_to_all(outbound.reshape(expert_groups * width_groups, width_group...]
    all_gather x3 -> x0, waiting for transfers between devices: 34.1 us -> none  [taken_in(): lax.all_gather(a, axis, axis=dim, tiled=True)]
    dot_general x3 -> x0, matrix products: 26.8 us -> none  [the longest x1 10.1 us: add_hidden(): jnp.dot(arrived_rows, pieces[0][0], preferred_element_type=jnp.float32)]
    gather x2 -> x0, local copies, waits for them, and re-layouts: 21.8 us -> none  [the longest x1 15.7 us: local(): picked = returned[row_index.reshape(-1)].astype(jnp.float32)]
    psum x1 -> x0, blocking collectives: 15 us -> none  [local(): total_sq = lax.psum(local_sq, 'tp')]
    another operation x2 -> x0, other arithmetic: 9.2 us -> none
  transfers between devices with their start and end apart: 4 -> 0, of which waited for: 3 -> 0; matrix products, arithmetic and copies ran while one was open for 15% -> 0% of each run, Pallas kernels for 0% -> 0%
where the time goes in v1:
time: 121 us; the launch traced here: 118 us
  Pallas kernels  117 us (97%)
  local copies, waits for them, and re-layouts  1.87 us (2%)
    pallas_call x1, Pallas kernels, local(): pl.pallas_call(kernel, out_shape=jax.ShapeDtypeStruct((NT * TOK, SL), BF1...  117 us

profile of v1, /device:TPU:2, one launch (start us, length us, event | category | flops | bytes accessed | tf_op | source)
XLA Modules:
  0.0 118.4 jit_solution(5864691906418078009)
XLA Ops:
  0.0 116.6 %shard_map.82 = bf16[1024,256]{1,0:T(8,128)(2,1)} custom-call(bf16[128,2048]{1,0:T(8,128)(2,1)} %tok_ref.1, s32[4,1024]{1,0:T(4,128)} %bitcast.4, f32[4,1024]{1,0:T(4,128)} %bitcast.5, f32[1,2048]{1,0:T(1,128)} %bitcast.6, bf16[1,2048,128]{2,1,0:T(8,128)(2,1)} %g_ref.1, bf16[1,2048,128]{2,1,0:T(8,128)(2,1)} %u_ref.1, bf16[1,128,2048]{2,1,0:T(8,128)(2,1)} %d_ref.1, ...), custom_call_target="tpu_custom_call" | custom-call | tf_op jit(solution)/shard_map/pallas_call | solution.py:377
  116.6 1.9 %copy.10 = bf16[1024,256]{1,0:T(8,128)(2,1)} copy(bf16[1024,256]{1,0:T(8,128)(2,1)} %shard_map.82) | data formatting | bytes 1048576
